TPU v7x, 32 devices: a whole 2x2x4 slice. The times are simulated.
32 devices in a mesh: dp: 4 (over y, x), kv: 4 (over z), tp: 2 (over core).
Axes of the slice: x: 2, y: 2, z: 4, core: 2. Of those that a mesh axis runs over, the one named last changes fastest.
Arguments:
- tokens: bfloat16 [4, 1024, 1024], P('dp', 'kv', 'tp'), may hold values from -6 to 6
- norm_gain: float32 [1024], replicated, may hold values from 0.1 to 1.9
- w_query: bfloat16 [1024, 1024], P(None, 'tp'), may hold values from -0.1875 to 0.1875
- w_key: bfloat16 [1024, 256], P(None, 'tp'), may hold values from -0.1875 to 0.1875
- w_value: bfloat16 [1024, 256], P(None, 'tp'), may hold values from -0.1875 to 0.1875
- q_gain: float32 [64], replicated, may hold values from 0.1 to 1.9
- k_gain: float32 [64], replicated, may hold values from 0.1 to 1.9
- w_out: bfloat16 [1024, 1024], P('tp'), may hold values from -4 to 4
- chosen: int32 [4, 32, 16], P('dp', 'kv'), may hold values from -1 to 31, as said below
Outputs:
- mixed: bfloat16 [4, 1024, 1024], P('dp', 'kv', 'tp')
- log_total: float32 [4, 16, 1024], P('dp', 'tp', 'kv')
Inputs may be any that keep to these rules, and one draw needn't show every extreme that they name: Each row of chosen (one query block b) holds distinct key block numbers, all at most b, and -1 for empty entries; b itself is always present; a row is full (16 blocks) whenever at least 16 blocks may be chosen by it. Over the 8 rows of one index of kv, the chosen blocks that lie on any one other index of kv are at most 4 distinct ones, and exactly 4 of those on the index just before, for every index but the first. Some blocks are chosen far more often than others.
All inputs are finite; a program needn't handle non-finite values.
Results may differ from a plain program's by a relative error of at most 0.015.
Values may be sent and summed in bfloat16 or wider, within the bound.
A program may use at most 64 MiB of HBM per device.

v0:
```python
import math

import jax
import jax.numpy as jnp
from jax import lax
from jax.sharding import PartitionSpec as P

H = 16
HD = 64
BLK = 32


epsilon = 1e-06
alibi_reach = 4.0
masked = -1e30


def rms_norm(values, gain):
    return (
        values
        * lax.rsqrt(jnp.mean(values * values, axis=-1, keepdims=True) + epsilon)
        * gain.astype(jnp.float32)
    )


def shards(tokens, norm_gain, w_query, w_key, w_value, q_gain, k_gain, w_out, chosen):
    gathered = lax.all_gather(tokens, "tp", axis=2, tiled=True)
    seq_dev, tok_dev, model_width = gathered.shape
    n_kv = lax.axis_size("kv")
    n_tp = lax.axis_size("tp")
    kv_index = lax.axis_index("kv")
    tp_index = lax.axis_index("tp")
    heads_here = w_query.shape[1] // HD
    kv_here = w_key.shape[1] // HD
    group_size = heads_here // kv_here
    blocks_here = tok_dev // BLK
    seq_len = tok_dev * n_kv
    hidden = (
        rms_norm(gathered.astype(jnp.float32), norm_gain)
        .astype(jnp.bfloat16)
        .reshape(seq_dev * tok_dev, model_width)
    )
    queries = rms_norm(
        jnp.dot(hidden, w_query, preferred_element_type=jnp.float32).reshape(
            seq_dev, tok_dev, heads_here, HD
        ),
        q_gain,
    ).astype(jnp.bfloat16)
    key_rows = rms_norm(
        jnp.dot(hidden, w_key, preferred_element_type=jnp.float32).reshape(
            seq_dev, tok_dev, kv_here, HD
        ),
        k_gain,
    ).astype(jnp.bfloat16)
    value_rows = (
        jnp.dot(hidden, w_value, preferred_element_type=jnp.float32)
        .astype(jnp.bfloat16)
        .reshape(seq_dev, tok_dev, kv_here, HD)
    )
    queries = queries.reshape(seq_dev, blocks_here, BLK, kv_here, group_size, HD)
    head_ids = tp_index * heads_here + jnp.arange(heads_here, dtype=jnp.int32)
    slopes = jnp.exp2(-8.0 * (head_ids + 1).astype(jnp.float32) / H).reshape(kv_here, group_size)
    query_pos = (kv_index * tok_dev + jnp.arange(tok_dev, dtype=jnp.int32)).reshape(
        blocks_here, BLK
    )
    score_scale = HD ** (-0.5)

    def absorb(state_now, span_keys, span_values, key_pos, usable):
        row_max, row_sum, weighted = state_now
        key_block = key_pos // BLK
        member = jnp.any(chosen[:, :, :, None] == key_block[:, None, None, :], axis=2)
        offset = query_pos[None, :, :, None] - key_pos[:, None, None, :]
        allowed = member[:, :, None, :] & usable[:, None, None, :] & (offset >= 0)
        scores = (
            jnp.einsum(
                "sbqkgd,snkd->skgbqn", queries, span_keys, preferred_element_type=jnp.float32
            )
            * score_scale
        )
        penalty = (
            slopes[None, :, :, None, None, None]
            * offset.astype(jnp.float32)[:, None, None]
            * alibi_reach
            / seq_len
        )
        scores = jnp.where(allowed[:, None, None], scores - penalty, masked)
        new_max = jnp.maximum(row_max, jnp.max(scores, axis=-1))
        weights = jnp.where(allowed[:, None, None], jnp.exp(scores - new_max[..., None]), 0.0)
        shrink = jnp.exp(row_max - new_max)
        row_sum = row_sum * shrink + jnp.sum(weights, axis=-1)
        weighted = weighted * shrink[..., None] + jnp.einsum(
            "skgbqn,snkd->skgbqd",
            weights.astype(jnp.bfloat16),
            span_values,
            preferred_element_type=jnp.float32,
        )
        return (new_max, row_sum, weighted)

    stat_shape = (seq_dev, kv_here, group_size, blocks_here, BLK)
    initial = (
        jnp.full(stat_shape, masked, jnp.float32),
        jnp.zeros(stat_shape, jnp.float32),
        jnp.zeros(stat_shape + (HD,), jnp.float32),
    )

    def fold_piece(state_now, shard_piece, first_row):
        piece_keys, piece_values = shard_piece
        row_count = piece_keys.shape[1]
        span_len = math.gcd(row_count, tok_dev)

        def one_span(step_index, running):
            first_key = step_index * span_len
            span_keys = lax.dynamic_slice_in_dim(piece_keys, first_key, span_len, 1)
            span_values = lax.dynamic_slice_in_dim(piece_values, first_key, span_len, 1)
            key_pos = jnp.broadcast_to(
                first_row.astype(jnp.int32) + first_key + jnp.arange(span_len, dtype=jnp.int32),
                (seq_dev, span_len),
            )
            return absorb(
                running, span_keys, span_values, key_pos, jnp.ones((seq_dev, span_len), bool)
            )

        return lax.fori_loop(0, row_count // span_len, one_span, state_now)

    row_max, row_sum, weighted = fold_piece(
        initial,
        (
            lax.all_gather(key_rows, "kv", axis=1, tiled=True),
            lax.all_gather(value_rows, "kv", axis=1, tiled=True),
        ),
        jnp.int32(0),
    )
    attended = (weighted / row_sum[..., None]).transpose(0, 3, 4, 1, 2, 5)
    attended = attended.reshape(seq_dev * tok_dev, heads_here * HD).astype(jnp.bfloat16)
    log_total = (row_max + jnp.log(row_sum)).reshape(seq_dev, heads_here, tok_dev)
    own_rows = model_width // n_tp

    def project():
        out_cols = lax.slice_in_dim(w_out, 0, own_rows * lax.axis_size("tp"), axis=1)
        return jnp.dot(attended, out_cols, preferred_element_type=jnp.float32).T

    scattered = lax.psum_scatter(
        project().astype(jnp.bfloat16), "tp", scatter_dimension=0, tiled=True
    ).astype(jnp.float32)
    mixed = scattered.T.reshape(seq_dev, tok_dev, own_rows).astype(jnp.bfloat16)
    return (mixed, log_total)


def solution(mesh):
    in_specs = (
        P("dp", "kv", "tp"),
        P(),
        P(None, "tp"),
        P(None, "tp"),
        P(None, "tp"),
        P(),
        P(),
        P("tp", None),
        P("dp", "kv", None),
    )
    out_specs = (P("dp", "kv", "tp"), P("dp", "tp", "kv"))
    return jax.shard_map(shards, mesh=mesh, in_specs=in_specs, out_specs=out_specs, check_vma=False)
```

profile of v0, /device:TPU:19, one launch (start us, length us, event | category | flops | bytes accessed | tf_op | source)
XLA Modules:
  0.0 80.3 jit_solution(10249953948225324526)
XLA Ops:
  7.3 2.8 %all_gather.9 = bf16[1,256,1024]{2,1,0:T(8,128)(2,1)S(1)} all-gather(bf16[1,256,512]{2,1,0:T(8,128)(2,1)} %param.11), channel_id=1, replica_groups=mesh['dp'=4,'kv'=4,'tp'=2] {'tp'}, dimensions={2}, use_global_device_ids=true | all-gather | bytes 786432 | tf_op jit(solution)/shard_map/all_gather | solution.py:27
  10.1 0.2 fusion.20
  10.3 1.4 %convolution_convert_fusion.1 = bf16[256,128]{0,1:T(8,128)(2,1)S(1)} fusion(bf16[1024,128]{1,0:T(8,128)(2,1)} %param.15, bf16[1,256,1024]{2,1,0:T(8,128)(2,1)S(1)} %all_gather.9, f32[1024]{0:T(1024)} %param.12, f32[256]{0:T(256)S(1)} %add_rsqrt_fusion.2), kind=kOutput, calls=%fused_computation.39 | convolution fusion | flops 68190208 | bytes 857088 | tf_op jit(solution)/shard_map/dot_general | solution.py:56
  11.7 0.4 fusion.30
  12.2 11.0 %all_gather.10 = bf16[1,1024,2,64]{1,3,2,0:T(8,128)(2,1)} all-gather(bf16[1,256,2,64]{1,3,2,0:T(8,128)(2,1)S(1)} %multiply_convert_fusion), channel_id=1, replica_groups=mesh['dp'=4,'kv'=4,'tp'=2] {'kv'}, dimensions={1}, use_global_device_ids=true | all-gather | bytes 327680 | tf_op jit(solution)/shard_map/all_gather | solution.py:128
  23.3 10.8 %all_gather.11 = bf16[1,1024,2,64]{1,3,2,0:T(8,128)(2,1)S(1)} all-gather(bf16[1,256,2,64]{1,3,2,0:T(8,128)(2,1)S(1)} %bitcast.99), channel_id=1, replica_groups=mesh['dp'=4,'kv'=4,'tp'=2] {'kv'}, dimensions={1}, use_global_device_ids=true | all-gather | bytes 327680 | tf_op jit(solution)/shard_map/all_gather | solution.py:129
  34.1 1.3 %fusion.33 = (f32[256,512]{1,0:T(8,128)S(1)}, f32[256,512]{1,0:T(8,128)}) fusion(bf16[1024,512]{1,0:T(8,128)(2,1)S(1)} %copy-done, bf16[1,256,1024]{2,1,0:T(8,128)(2,1)S(1)} %all_gather.9, f32[1024]{0:T(1024)S(1)} %copy-done.3, f32[256]{0:T(256)S(1)} %add_rsqrt_fusion.2), kind=kOutput, calls=%fused_computation.59 | convolution fusion | flops 269615104 | bytes 2626560 | tf_op jit(solution)/shard_map/dot_general | solution.py:44
  35.3 0.2 copy.26
  35.7 1.6 %reshape.336 = f32[1,8,32,2,4,64]{5,4,3,2,1,0:T(4,128)S(1)} reshape(f32[256,512]{1,0:T(8,128)} %get-tuple-element.319) | data formatting | bytes 1048576 | tf_op jit(solution)/shard_map/reshape | solution.py:44
  37.3 1.1 %fusion.24 = bf16[1,8,32,2,4,64]{5,2,4,1,3,0:T(8,128)(2,1)} fusion(f32[1,8,32,2,4,64]{5,4,3,2,1,0:T(4,128)S(1)} %reshape.336, f32[64]{0:T(128)S(1)} %copy-done.5, f32[8,32,2,4]{1,3,0,2:T(4,128)S(1)} %copy.27), kind=kLoop, calls=%fused_computation.45 | loop fusion | flops 393216 | bytes 794880 | tf_op jit(solution)/shard_map/convert_element_type | solution.py:48
  38.4 15.7 %while.20 = (s32[]{:T(128)}, f32[1,2,4,8,32]{4,2,3,1,0:T(4,128)S(1)}, f32[1,2,4,8,32]{4,2,3,1,0:T(4,128)S(1)}, f32[1,2,4,8,32,64]{5,4,3,2,1,0:T(8,128)S(1)}, s32...) while((s32[]{:T(128)}, ...), condition=%wide.region_7.8_spmd.clone, body=%wide.region_3.7_spmd.clone.sunk | while | flops 140261664 | bytes 9419611 | solution.py:123
  38.7 0.1 fusion.48
  39.0 1.7 %fusion.49 = (f32[2,4,8,32]{3,1,2,0:T(4,128)S(1)}, f32[1,2,4,8,32,256]{5,4,2,3,1,0:T(8,128)S(1)}) fusion(f32[8,32,256]{2,1,0:T(8,128)S(1)} %subtract_convert_fusion.2, f32[2,4]{1,0:T(2,128)S(1)} %mul.331, bf16[1,8,32,2,4,64]{5,2,4,1,3,0:T(8,128)(2,1)} %get-tuple-element.431, bf16[1,1024,2,64]{1,3,2,0:T(8,128)(2,1)} %get-tuple-element.430, ...), kind=kOutput, calls=%fused_computation.58.clone.1 | convolution fusion | flops 70252544 | bytes 3022884 | tf_op jit(solution)/shard_map/while/body/eval_jaxpr/sbqkgd,snkd->skgbqn/dot_general | solution.py:75
  40.8 0.8 %fusion.51 = (bf16[2,4,8,32,256]{4,3,1,2,0:T(8,128)(2,1)S(1)}, f32[2,4,8,32]{3,1,2,0:T(4,128)S(1)}) fusion(f32[1,2,4,8,32,256]{5,4,2,3,1,0:T(8,128)S(1)} %get-tuple-element.393, f32[2,4,8,32]{3,1,2,0:T(4,128)S(1)} %bitcast.92, pred[8,32,256]{2,1,0:T(8,128)(4,1)S(1)} %fusion.48), kind=kLoop, calls=%fused_computation.9.clone.1 | loop fusion | flops 2095104 | bytes 3227648 | tf_op jit(solution)/shard_map/reshape.263
  41.7 0.6 fusion.52
  42.7 0.1 fusion.48
  42.9 1.7 %fusion.49 = (f32[2,4,8,32]{3,1,2,0:T(4,128)S(1)}, f32[1,2,4,8,32,256]{5,4,2,3,1,0:T(8,128)S(1)}) fusion(f32[8,32,256]{2,1,0:T(8,128)S(1)} %subtract_convert_fusion.2, f32[2,4]{1,0:T(2,128)S(1)} %mul.331, bf16[1,8,32,2,4,64]{5,2,4,1,3,0:T(8,128)(2,1)} %get-tuple-element.431, bf16[1,1024,2,64]{1,3,2,0:T(8,128)(2,1)} %get-tuple-element.430, ...), kind=kOutput, calls=%fused_computation.58.clone.1 | convolution fusion | flops 70252544 | bytes 3022884 | tf_op jit(solution)/shard_map/while/body/eval_jaxpr/sbqkgd,snkd->skgbqn/dot_general | solution.py:75
  44.7 0.8 %fusion.51 = (bf16[2,4,8,32,256]{4,3,1,2,0:T(8,128)(2,1)S(1)}, f32[2,4,8,32]{3,1,2,0:T(4,128)S(1)}) fusion(f32[1,2,4,8,32,256]{5,4,2,3,1,0:T(8,128)S(1)} %get-tuple-element.393, f32[2,4,8,32]{3,1,2,0:T(4,128)S(1)} %bitcast.92, pred[8,32,256]{2,1,0:T(8,128)(4,1)S(1)} %fusion.48), kind=kLoop, calls=%fused_computation.9.clone.1 | loop fusion | flops 2095104 | bytes 3227648 | tf_op jit(solution)/shard_map/reshape.263
  45.6 0.7 fusion.52
  46.6 0.1 fusion.48
  46.8 1.7 %fusion.49 = (f32[2,4,8,32]{3,1,2,0:T(4,128)S(1)}, f32[1,2,4,8,32,256]{5,4,2,3,1,0:T(8,128)S(1)}) fusion(f32[8,32,256]{2,1,0:T(8,128)S(1)} %subtract_convert_fusion.2, f32[2,4]{1,0:T(2,128)S(1)} %mul.331, bf16[1,8,32,2,4,64]{5,2,4,1,3,0:T(8,128)(2,1)} %get-tuple-element.431, bf16[1,1024,2,64]{1,3,2,0:T(8,128)(2,1)} %get-tuple-element.430, ...), kind=kOutput, calls=%fused_computation.58.clone.1 | convolution fusion | flops 70252544 | bytes 3022884 | tf_op jit(solution)/shard_map/while/body/eval_jaxpr/sbqkgd,snkd->skgbqn/dot_general | solution.py:75
  48.6 0.8 %fusion.51 = (bf16[2,4,8,32,256]{4,3,1,2,0:T(8,128)(2,1)S(1)}, f32[2,4,8,32]{3,1,2,0:T(4,128)S(1)}) fusion(f32[1,2,4,8,32,256]{5,4,2,3,1,0:T(8,128)S(1)} %get-tuple-element.393, f32[2,4,8,32]{3,1,2,0:T(4,128)S(1)} %bitcast.92, pred[8,32,256]{2,1,0:T(8,128)(4,1)S(1)} %fusion.48), kind=kLoop, calls=%fused_computation.9.clone.1 | loop fusion | flops 2095104 | bytes 3227648 | tf_op jit(solution)/shard_map/reshape.263
  49.5 0.7 fusion.52
  50.8 1.7 %fusion.49 = (f32[2,4,8,32]{3,1,2,0:T(4,128)S(1)}, f32[1,2,4,8,32,256]{5,4,2,3,1,0:T(8,128)S(1)}) fusion(f32[8,32,256]{2,1,0:T(8,128)S(1)} %subtract_convert_fusion.2, f32[2,4]{1,0:T(2,128)S(1)} %mul.331, bf16[1,8,32,2,4,64]{5,2,4,1,3,0:T(8,128)(2,1)} %get-tuple-element.431, bf16[1,1024,2,64]{1,3,2,0:T(8,128)(2,1)} %get-tuple-element.430, ...), kind=kOutput, calls=%fused_computation.58.clone.1 | convolution fusion | flops 70252544 | bytes 3022884 | tf_op jit(solution)/shard_map/while/body/eval_jaxpr/sbqkgd,snkd->skgbqn/dot_general | solution.py:75
  52.6 0.8 %fusion.51 = (bf16[2,4,8,32,256]{4,3,1,2,0:T(8,128)(2,1)S(1)}, f32[2,4,8,32]{3,1,2,0:T(4,128)S(1)}) fusion(f32[1,2,4,8,32,256]{5,4,2,3,1,0:T(8,128)S(1)} %get-tuple-element.393, f32[2,4,8,32]{3,1,2,0:T(4,128)S(1)} %bitcast.92, pred[8,32,256]{2,1,0:T(8,128)(4,1)S(1)} %fusion.48), kind=kLoop, calls=%fused_computation.9.clone.1 | loop fusion | flops 2095104 | bytes 3227648 | tf_op jit(solution)/shard_map/reshape.263
  53.5 0.7 fusion.52
  54.2 0.3 fusion.26
  54.5 0.4 copy.30
  54.9 0.3 convert_element_type.92
  55.4 1.2 %fusion.19 = bf16[1024,256]{0,1:T(8,128)(2,1)} fusion(bf16[256,512]{1,0:T(8,128)(2,1)S(1)} %convert_element_type.92, bf16[512,1024]{1,0:T(8,128)(2,1)S(1)} %copy-done.1), kind=kOutput, calls=%fused_computation.38 | convolution fusion | flops 268697600 | bytes 1835008 | tf_op jit(solution)/shard_map/dot_general | solution.py:140
  56.7 0.7 reshape.338
  57.3 16.1 %reduce-scatter.2.cloned.1.call-done = bf16[512,256]{0,1:T(8,128)(2,1)} async-done(((bf16[1024,256]{0,1:T(8,128)(2,1)}), bf16[512,256]{0,1:T(8,128)(2,1)}) %reduce-scatter.2.cloned.1.call-update) | async-done | bytes 262160 | tf_op jit(solution)/shard_map/reduce_scatter | solution.py:142
  (75 shorter events, 2.5 us)
Async XLA Ops:
  7.2 26.9 %copy-start = (bf16[1024,512]{1,0:T(8,128)(2,1)S(1)}, bf16[1024,512]{1,0:T(8,128)(2,1)}, u32[]{:S(2)}) copy-start(bf16[1024,512]{1,0:T(8,128)(2,1)} %param.13) | copy-start | bytes 3145732
  7.2 4.5 %copy-start.3 = (f32[1024]{0:T(1024)S(1)}, f32[1024]{0:T(1024)}, u32[]{:S(2)}) copy-start(f32[1024]{0:T(1024)} %param.12) | copy-start | bytes 12292
  7.2 4.5 %copy-start.6 = (bf16[1024,128]{1,0:T(8,128)(2,1)S(1)}, bf16[1024,128]{1,0:T(8,128)(2,1)}, u32[]{:S(2)}) copy-start(bf16[1024,128]{1,0:T(8,128)(2,1)} %param.14) | copy-start | bytes 786436
  7.2 4.9 %copy-start.4 = (f32[64]{0:T(128)S(1)}, f32[64]{0:T(128)}, u32[]{:S(2)}) copy-start(f32[64]{0:T(128)} %param.17) | copy-start | bytes 772
  7.2 66.2 %reduce-scatter.2.cloned.1.call-start = ((), (), s32[]{:S(2)}) async-start(), calls=%async_computation.1 | async-start | bytes 786432 | tf_op jit(solution)/shard_map/reduce_scatter | solution.py:142
  35.3 2.0 %copy-start.5 = (f32[64]{0:T(128)S(1)}, f32[64]{0:T(128)}, u32[]{:S(2)}) copy-start(f32[64]{0:T(128)} %param.16) | copy-start | bytes 772
  35.5 2.9 %copy-start.2 = (s32[1,8,16]{2,1,0:T(8,128)S(1)}, s32[1,8,16]{2,1,0:T(8,128)}, u32[]{:S(2)}) copy-start(s32[1,8,16]{2,1,0:T(8,128)} %param.19) | copy-start | bytes 1540
  54.1 1.2 %copy-start.1 = (bf16[512,1024]{1,0:T(8,128)(2,1)S(1)}, bf16[512,1024]{1,0:T(8,128)(2,1)}, u32[]{:S(2)}) copy-start(bf16[512,1024]{1,0:T(8,128)(2,1)} %param.18) | copy-start | bytes 3145732
Sparse Core Ops, SparseCore 0:
  56.7 16.6 reduce-scatter.1
where the time goes:
time: 81.6 us; the launch traced here: 80.3 us
  blocking collectives  24.7 us (30%)
  waiting for transfers between devices  16.1 us (20%)
  between operations  14.3 us (18%)
  matrix products  13.9 us (17%)
  other arithmetic  6.91 us (8%)
  local copies, waits for them, and re-layouts  4.09 us (5%)
    reduce_scatter x1, waiting for transfers between devices, shards(): lax.psum_scatter(project().astype(jnp.bfloat16), 'tp', scatter_dimension=...  16.1 us
    all_gather x1, blocking collectives, shards(): lax.all_gather(key_rows, 'kv', axis=1, tiled=True)  11 us
    all_gather x1, blocking collectives, shards(): lax.all_gather(value_rows, 'kv', axis=1, tiled=True)  10.8 us
    dot_general x4, matrix products, absorb(): jnp.einsum('sbqkgd,snkd->skgbqn', queries, span_keys, preferred_element_t...  6.99 us
    another operation x4, other arithmetic  3.32 us
    all_gather x1, blocking collectives, shards(): gathered = lax.all_gather(tokens, 'tp', axis=2, tiled=True)  2.83 us
    dot_general x4, matrix products, absorb(): jnp.einsum('skgbqn,snkd->skgbqd', weights.astype(jnp.bfloat16), span_valu...  2.63 us
  transfers between devices with their start and end apart: 1, of which 1 were waited for; matrix products, arithmetic and copies ran while one was open for 1% of the time, Pallas kernels for 0%

commit v1 on v0

v1 whole, which is shorter than its diff:
```python
import functools
import math

import jax
import jax.numpy as jnp
from jax import lax
from jax.experimental import pallas as pl
from jax.experimental.pallas import tpu as pltpu
from jax.sharding import PartitionSpec as P

HD = 64
BLK = 32
MOST = 4
LANES = 128
PIECES = 3

epsilon = 1e-06
alibi_reach = 4.0
masked = -1e30
LOG2E = math.log2(math.e)
F32 = jnp.float32
BF16 = jnp.bfloat16
NT = (((1,), (1,)), ((), ()))


def iota(shape, dim):
    return lax.broadcasted_iota(jnp.int32, shape, dim)


def dot(a, b):
    return jnp.dot(a, b, preferred_element_type=F32)


def dot_nt(a, b):
    return lax.dot_general(a, b, NT, preferred_element_type=F32)


def kernel(
    n_kv,
    tok, gain, wq, wk, wv, qg, kg, wo, ch,
    out_ref, lt_ref,
    x_buf, ch_buf, w_buf, wo_buf, g_buf, qg_buf, kg_buf,
    q_s, kv_s, send_s, recv_s, acc, part_send, part_recv,
    load_sem, x_sem, ch_sem, kv_sem, part_sem,
):
    me = lax.axis_index("kv")
    tp = lax.axis_index("tp")
    partner = 1 - tp
    rows, half = tok.shape
    q_cols = wq.shape[1]
    k_cols = wk.shape[1]
    heads = q_cols // HD
    kv_heads = k_cols // HD
    group = heads // kv_heads
    n_heads = heads * lax.axis_size("tp")
    nb = ch.shape[0]
    entries = ch.shape[1]
    nbp = -(-n_kv * nb // LANES) * LANES
    picked = MOST * BLK
    width = half * 2
    seq_len = rows * n_kv
    alibi = alibi_reach / seq_len

    def span(start):
        return pl.ds(pl.multiple_of(start * half, LANES), half)

    loads = {}

    def load(name, pos, src, dst):
        copy = pltpu.make_async_copy(src, dst, load_sem.at[pos])
        copy.start()
        loads[name] = copy

    load("tok", 0, tok, x_buf.at[0])
    load("ch", 1, ch, ch_buf.at[me])
    load("g0", 2, gain.at[:, span(tp)], g_buf.at[0])
    load("g1", 3, gain.at[:, span(partner)], g_buf.at[1])
    load("qg", 4, qg, qg_buf)
    load("kg", 5, kg, kg_buf)
    for side, which in ((0, tp), (1, partner)):
        load(f"wq{side}", 6 + side, wq.at[span(which), :], w_buf.at[side, :, 0:q_cols])
        load(f"wk{side}", 8 + side, wk.at[span(which), :], w_buf.at[side, :, q_cols:q_cols + k_cols])
        load(f"wv{side}", 10 + side, wv.at[span(which), :], w_buf.at[side, :, q_cols + k_cols:q_cols + 2 * k_cols])
    for side, which in ((0, tp), (1, partner)):
        load(f"wo{side}", 12 + side, wo.at[:, span(which)], wo_buf.at[side])

    def peers(step):
        lax.fori_loop(1, n_kv, lambda d, c: (step(d), c)[1], 0, unroll=n_kv <= 8)

    barrier = pltpu.get_barrier_semaphore()
    pl.semaphore_signal(barrier, inc=1, device_id={"tp": partner}, device_id_type=pl.DeviceIdType.MESH)
    peers(lambda d: pl.semaphore_signal(
        barrier, inc=1, device_id={"kv": lax.rem(me + d, n_kv)}, device_id_type=pl.DeviceIdType.MESH))

    loads["tok"].wait()
    loads["ch"].wait()
    pl.semaphore_wait(barrier, n_kv)

    x_copy = pltpu.make_async_remote_copy(
        x_buf.at[0], x_buf.at[1], x_sem.at[0], x_sem.at[1],
        device_id={"tp": partner}, device_id_type=pl.DeviceIdType.MESH)
    x_copy.start()

    def list_copy(owner, target):
        return pltpu.make_async_remote_copy(
            ch_buf.at[owner], ch_buf.at[owner], ch_sem.at[0, target], ch_sem.at[1, owner],
            device_id={"kv": target}, device_id_type=pl.DeviceIdType.MESH)

    def send_list(d):
        @pl.when(me - d >= 0)
        def _():
            list_copy(me, lax.max(me - d, 0)).start()

    peers(send_list)

    def scaled(side):
        x = x_buf[side].astype(F32)
        return (x * g_buf[side]).astype(BF16), jnp.sum(x * x, axis=1, keepdims=True)

    for name in ("g0", "g1", "qg", "kg", "wq0", "wk0", "wv0"):
        loads[name].wait()
    y0, sq0 = scaled(0)
    raw = dot(y0, w_buf[0])
    for name in ("wq1", "wk1", "wv1"):
        loads[name].wait()
    x_copy.wait()
    y1, sq1 = scaled(1)
    raw = (raw + dot(y1, w_buf[1])) * lax.rsqrt((sq0 + sq1) / width + epsilon)

    same_head = jnp.where(
        iota((LANES, LANES), 0) // HD == iota((LANES, LANES), 1) // HD, 1.0, 0.0).astype(BF16)

    def head_norm(v, gain_row):
        sq = v * v
        hi = sq.astype(BF16)
        lo = (sq - hi.astype(F32)).astype(BF16)
        total = dot(hi, same_head) + dot(lo, same_head)
        return v * lax.rsqrt(total / HD + epsilon) * gain_row

    qg_row = jnp.concatenate([qg_buf[...], qg_buf[...]], axis=1) * (HD ** -0.5 * LOG2E)
    kg_row = jnp.concatenate([kg_buf[...], kg_buf[...]], axis=1)
    for tile in range(k_cols // LANES):
        at = tile * LANES
        kv_s[:, at:at + LANES] = head_norm(
            raw[:, q_cols + at:q_cols + at + LANES], kg_row).astype(BF16)
    kv_s[:, k_cols:] = raw[:, q_cols + k_cols:].astype(BF16)

    lane_block = iota((nb, nbp), 1)

    def member_of(lists):
        hit = lists[:, 0:1] == lane_block
        for e in range(1, entries):
            hit = hit | (lists[:, e:e + 1] == lane_block)
        return jnp.where(hit, 1.0, 0.0)

    before = jnp.where(
        (iota((nbp, nbp), 0) < iota((nbp, nbp), 1))
        & (iota((nbp, nbp), 0) // nb == iota((nbp, nbp), 1) // nb), 1.0, 0.0).astype(BF16)

    def need_and_rank(member):
        need = jnp.broadcast_to(jnp.max(member, axis=0, keepdims=True), (8, nbp))
        return need[0:1], dot(need.astype(BF16), before)[0:1]

    slot = (iota((picked, nbp), 0) // BLK).astype(F32)
    lane_owner = iota((picked, nbp), 1) // nb

    def one_hot(need, rank, owner):
        return jnp.where(
            (need > 0.5) & (rank == slot) & (lane_owner == owner), 1.0, 0.0).astype(BF16)

    spread = jnp.where(
        iota((nbp, rows), 0) == me * nb + iota((nbp, rows), 1) // BLK, 1.0, 0.0).astype(BF16)
    same_row = iota((picked, rows), 0) % BLK == iota((picked, rows), 1) % BLK

    def kv_copy(owner, target):
        return pltpu.make_async_remote_copy(
            send_s.at[target], recv_s.at[owner], kv_sem.at[0, target], kv_sem.at[1, owner],
            device_id={"kv": target}, device_id_type=pl.DeviceIdType.MESH)

    def send_rows(step):
        d = n_kv - step

        @pl.when(me + d < n_kv)
        def _():
            target = lax.min(me + d, n_kv - 1)
            list_copy(target, me).wait_recv()
            need, rank = need_and_rank(member_of(ch_buf[target]))
            chosen_rows = jnp.where(same_row, dot(one_hot(need, rank, me), spread), 0.0)
            send_s[target] = dot(chosen_rows.astype(BF16), kv_s[...]).astype(BF16)
            kv_copy(me, target).start()

    peers(send_rows)

    lane_q = iota((rows, LANES), 1)
    row_q = iota((rows, LANES), 0)
    own_block = jnp.where(lane_q - HD == row_q // BLK, 1.0, 0.0)

    def slope_of(head):
        return jnp.exp2(-8.0 / n_heads * (tp * heads + head + 1).astype(F32))

    def lane_fill(base, first, value):
        return jnp.where(lane_q == first, value, base)

    for tile in range(q_cols // LANES):
        at = tile * LANES
        q = head_norm(raw[:, at:at + LANES], qg_row)
        for odd in range(2):
            head = 2 * tile + odd
            value = slope_of(jnp.full((rows, LANES), head, jnp.int32)) * (alibi * LOG2E)
            extra = own_block
            for piece in range(PIECES):
                part = value.astype(BF16).astype(F32)
                value = value - part
                extra = lane_fill(extra, HD + nb + piece, part * BLK)
                extra = lane_fill(extra, HD + nb + PIECES + piece, part)
            here = q if odd == 0 else pltpu.roll(q, HD, 1)
            q_s[head] = jnp.where(lane_q < HD, here, extra).astype(BF16)

    member = member_of(ch_buf[me])
    relative = (lane_block - me * nb).astype(F32)
    pieces_rows = jnp.where(
        iota((8, nbp), 0) < PIECES,
        jnp.broadcast_to(relative[0:1], (8, nbp)), 0.0)
    table = jnp.concatenate(
        [jnp.zeros((HD, nbp), F32), member, pieces_rows,
         jnp.zeros((LANES - HD - nb - 8, nbp), F32)], axis=0).astype(BF16)

    def key_extra(hot):
        count = hot.shape[0]
        lane = iota((count, LANES), 1)
        found = dot_nt(hot, table)
        inside = (iota((count, LANES), 0) % BLK).astype(F32)
        tail = jnp.where(lane < HD + nb + 2 * PIECES, inside, 0.0)
        tail = jnp.where(lane < HD + nb + PIECES, found, tail)
        return jnp.where(lane < HD + nb, (found - 1.0) * -masked, tail)

    def attend(load_tile, extra, causal, first):
        count = extra.shape[0]
        low = iota((count, LANES), 1) < HD
        for g in range(kv_heads):
            at = g * HD // LANES * LANES
            k = load_tile(at).astype(F32)
            v = load_tile(k_cols + at).astype(F32)
            if g % 2:
                k = pltpu.roll(k, HD, 1)
                v = pltpu.roll(v, HD, 1)
            k = jnp.where(low, k, extra).astype(BF16)
            v = jnp.where(low, v, 1.0).astype(BF16)
            for h in range(g * group, (g + 1) * group):
                weights = jnp.exp2(dot_nt(q_s[h], k))
                if causal is not None:
                    weights = jnp.where(causal, weights, 0.0)
                add = dot(weights.astype(BF16), v)
                if first:
                    acc[h] = add
                else:
                    acc[h] += add

    hot_own = jnp.where(
        iota((rows, nbp), 1) == me * nb + iota((rows, nbp), 0) // BLK, 1.0, 0.0).astype(BF16)
    causal = iota((rows, rows), 1) <= iota((rows, rows), 0)
    attend(lambda at: kv_s[:, at:at + LANES], key_extra(hot_own), causal, True)

    need_own, rank_own = need_and_rank(member)

    def absorb(d):
        @pl.when(me - d >= 0)
        def _():
            owner = lax.max(me - d, 0)
            extra = key_extra(one_hot(need_own, rank_own, owner))
            kv_copy(owner, me).wait_recv()
            attend(lambda at: recv_s[owner, :, at:at + LANES], extra, None, False)

    peers(absorb)

    sums = jnp.ones((rows, LANES), F32)
    tiles = []
    for tile in range(q_cols // LANES):
        sides = []
        for odd in range(2):
            head = 2 * tile + odd
            o = acc[head]
            total = pltpu.roll(o, HD, 1)
            sums = jnp.where(lane_q == head, total, sums)
            sides.append(o / total)
        tiles.append(jnp.where(lane_q < HD, sides[0], pltpu.roll(sides[1], HD, 1)))
    attended = jnp.concatenate(tiles, axis=1).astype(BF16)

    loads["wo1"].wait()
    part_send[...] = dot(attended, wo_buf[1]).astype(BF16)
    part_copy = pltpu.make_async_remote_copy(
        part_send, part_recv, part_sem.at[0], part_sem.at[1],
        device_id={"tp": partner}, device_id_type=pl.DeviceIdType.MESH)
    part_copy.start()
    loads["wo0"].wait()
    own = dot(attended, wo_buf[0])
    logs = jnp.log(sums) - slope_of(lane_q) * alibi * row_q.astype(F32)
    lt_ref[...] = logs.T[0:heads]

    def finish(d):
        @pl.when(me + d < n_kv)
        def _():
            kv_copy(me, lax.min(me + d, n_kv - 1)).wait_send()

        @pl.when(me - d >= 0)
        def _():
            list_copy(me, lax.max(me - d, 0)).wait_send()

    peers(finish)
    part_copy.wait()
    out_ref[...] = (own + part_recv[...].astype(F32)).astype(BF16)


def shards(n_kv, tokens, norm_gain, w_query, w_key, w_value, q_gain, k_gain, w_out, chosen):
    seqs, rows, half = tokens.shape
    nb, entries = chosen.shape[1:]
    q_cols, k_cols = w_query.shape[1], w_key.shape[1]
    heads = q_cols // HD
    vmem = pltpu.VMEM
    dma = pltpu.SemaphoreType.DMA
    mixed, log_total = pl.pallas_call(
        functools.partial(kernel, n_kv),
        out_shape=(
            jax.ShapeDtypeStruct((rows, half), BF16),
            jax.ShapeDtypeStruct((heads, rows), F32),
        ),
        in_specs=[pl.BlockSpec(memory_space=pl.ANY)] * 9,
        out_specs=(pl.BlockSpec(memory_space=vmem), pl.BlockSpec(memory_space=vmem)),
        scratch_shapes=[
            vmem((2, rows, half), BF16),
            vmem((n_kv, nb, entries), jnp.int32),
            vmem((2, half, q_cols + 2 * k_cols), BF16),
            vmem((2, q_cols, half), BF16),
            vmem((2, 1, half), F32),
            vmem((1, HD), F32),
            vmem((1, HD), F32),
            vmem((heads, rows, LANES), BF16),
            vmem((rows, 2 * k_cols), BF16),
            vmem((n_kv, MOST * BLK, 2 * k_cols), BF16),
            vmem((n_kv, MOST * BLK, 2 * k_cols), BF16),
            vmem((heads, rows, LANES), F32),
            vmem((rows, half), BF16),
            vmem((rows, half), BF16),
            dma((14,)),
            dma((2,)),
            dma((2, n_kv)),
            dma((2, n_kv)),
            dma((2,)),
        ],
        compiler_params=pltpu.CompilerParams(
            collective_id=0, has_side_effects=True, vmem_limit_bytes=48 * 1024 * 1024
        ),
    )(
        tokens.reshape(rows, half), norm_gain.reshape(1, -1), w_query, w_key, w_value,
        q_gain.reshape(1, -1), k_gain.reshape(1, -1), w_out, chosen.reshape(nb, entries),
    )
    return mixed.reshape(seqs, rows, half), log_total.reshape(seqs, heads, rows)


def solution(mesh):
    in_specs = (
        P("dp", "kv", "tp"),
        P(),
        P(None, "tp"),
        P(None, "tp"),
        P(None, "tp"),
        P(),
        P(),
        P("tp", None),
        P("dp", "kv", None),
    )
    out_specs = (P("dp", "kv", "tp"), P("dp", "tp", "kv"))
    return jax.shard_map(
        functools.partial(shards, mesh.shape["kv"]),
        mesh=mesh, in_specs=in_specs, out_specs=out_specs, check_vma=False)
```

time: 81.6 us -> 25.3 us (0.31); the launches traced: 80.3 us -> 25 us
  blocking collectives: 24.7 us -> 0 us
  Pallas kernels: 0 us -> 17.1 us
  waiting for transfers between devices: 16.1 us -> 0 us
  matrix products: 13.9 us -> 0 us
  between operations: 14.3 us -> 0.68 us
  other arithmetic: 6.91 us -> 0 us
  local copies, waits for them, and re-layouts: 4.09 us -> 7.28 us
    all_gather x3 -> x0, blocking collectives: 24.7 us -> none  [the longest x1 11 us: shards(): lax.all_gather(key_rows, 'kv', axis=1, tiled=True)]
    pallas_call x0 -> x1, Pallas kernels: none -> 17.1 us  [shards(): pl.pallas_call(functools.partial(kernel, n_kv), out_shape=(jax.ShapeDtype...]
    reduce_scatter x1 -> x0, waiting for transfers between devices: 16.1 us -> none  [shards(): lax.psum_scatter(project().astype(jnp.bfloat16), 'tp', scatter_dimension=...]
    dot_general x12 -> x0, matrix products: 13.9 us -> none  [the longest x4 6.99 us: absorb(): jnp.einsum('sbqkgd,snkd->skgbqn', queries, span_keys, preferred_element_t...]
    unnamed x14 -> x20, local copies, waits for them, and re-layouts: 0.15 us -> 7.28 us
    another operation x4 -> x0, other arithmetic: 3.32 us -> none
    reshape x2 -> x0, local copies, waits for them, and re-layouts: 2.26 us -> none  [the longest x1 1.59 us: shards(): jnp.dot(hidden, w_query, preferred_element_type=jnp.float32)]
    convert_element_type x7 -> x0, other arithmetic: 1.95 us -> none  [the longest x1 1.13 us: shards(): queries = rms_norm(jnp.dot(hidden, w_query, preferred_element_type=jnp.fl...]
  transfers between devices with their start and end apart: 1 -> 0, of which waited for: 1 -> 0; matrix products, arithmetic and copies ran while one was open for 1% -> 0% of each run, Pallas kernels for 0% -> 0%
where the time goes in v1:
time: 25.3 us; the launch traced here: 25 us
  Pallas kernels  17.1 us (68%)
  local copies, waits for them, and re-layouts  7.28 us (29%)
  between operations  0.68 us (3%)
    pallas_call x1, Pallas kernels, shards(): pl.pallas_call(functools.partial(kernel, n_kv), out_shape=(jax.ShapeDtype...  17.1 us
    unnamed x20, local copies, waits for them, and re-layouts  7.28 us

profile of v1, /device:TPU:19, one launch (start us, length us, event | category | flops | bytes accessed | tf_op | source)
XLA Modules:
  0.0 25.0 jit_solution(6661159669590234404)
XLA Ops:
  0.6 0.0 copy-start.6
  0.6 0.0 copy-start.5
  0.7 0.0 copy-start.7
  0.7 0.0 copy-start.8
  0.7 0.6 %copy-done.6 = s32[1,8,16]{2,1,0:T(8,128)S(1)} copy-done((s32[1,8,16]{2,1,0:T(8,128)S(1)}, s32[1,8,16]{2,1,0:T(8,128)}, u32[]{:S(2)}) %copy-start.6) | copy-done | bytes 536
  1.3 0.0 copy-done.5
  1.3 0.0 copy-done.7
  1.3 0.0 copy-done.8
  1.3 0.0 copy-start
  1.3 1.2 %copy-done = bf16[1024,512]{1,0:T(8,128)(2,1)S(1)} copy-done((bf16[1024,512]{1,0:T(8,128)(2,1)S(1)}, bf16[1024,512]{1,0:T(8,128)(2,1)}, u32[]{:S(2)}) %copy-start) | copy-done | bytes 1048600
  2.6 0.0 copy-start.1
  2.6 1.2 %copy-done.1 = bf16[512,1024]{1,0:T(8,128)(2,1)S(1)} copy-done((bf16[512,1024]{1,0:T(8,128)(2,1)S(1)}, bf16[512,1024]{1,0:T(8,128)(2,1)}, u32[]{:S(2)}) %copy-start.1) | copy-done | bytes 1048600
  3.8 0.0 copy-start.2
  3.8 0.9 %copy-done.2 = bf16[1,256,512]{2,1,0:T(8,128)(2,1)S(1)} copy-done((bf16[1,256,512]{2,1,0:T(8,128)(2,1)S(1)}, bf16[1,256,512]{2,1,0:T(8,128)(2,1)}, u32[]{:S(2)}) %copy-start.2) | copy-done | bytes 262168
  4.7 0.0 copy-start.3
  4.7 0.9 %copy-done.3 = bf16[1024,128]{1,0:T(8,128)(2,1)S(1)} copy-done((bf16[1024,128]{1,0:T(8,128)(2,1)S(1)}, bf16[1024,128]{1,0:T(8,128)(2,1)}, u32[]{:S(2)}) %copy-start.3) | copy-done | bytes 262168
  5.7 0.0 copy-start.4
  5.7 0.9 %copy-done.4 = bf16[1024,128]{1,0:T(8,128)(2,1)S(1)} copy-done((bf16[1024,128]{1,0:T(8,128)(2,1)S(1)}, bf16[1024,128]{1,0:T(8,128)(2,1)}, u32[]{:S(2)}) %copy-start.4) | copy-done | bytes 262168
  6.6 17.1 %shard_map.104 = (bf16[256,512]{1,0:T(8,128)(2,1)S(1)}, f32[8,256]{1,0:T(8,128)S(1)}) custom-call(bf16[256,512]{1,0:T(8,128)(2,1)S(1)} %bitcast.8, f32[1,1024]{1,0:T(1,128)S(1)} %bitcast.10, bf16[1024,512]{1,0:T(8,128)(2,1)S(1)} %copy-done, bf16[1024,128]{1,0:T(8,128)(2,1)S(1)} %copy-done.3, bf16[1024,128]{1,0:T(8,128)(2,1)S(1)} %copy-done.4, ...), custom_call_target="tpu_custom_call" | custom-call | tf_op jit(solution)/shard_map/pallas_call | solution.py:321
  23.7 0.7 %copy.13 = bf16[1,256,512]{2,1,0:T(8,128)(2,1)} copy(bf16[1,256,512]{2,1,0:T(8,128)(2,1)S(1)} %bitcast.7) | data formatting | bytes 524288
  24.4 0.6 %copy.14 = f32[1,8,256]{2,1,0:T(8,128)} copy(f32[1,8,256]{2,1,0:T(8,128)S(1)} %bitcast.9) | data formatting | bytes 16384
Async XLA Ops:
  0.6 0.7 %copy-start.6 = (s32[1,8,16]{2,1,0:T(8,128)S(1)}, s32[1,8,16]{2,1,0:T(8,128)}, u32[]{:S(2)}) copy-start(s32[1,8,16]{2,1,0:T(8,128)} %param.17) | copy-start | bytes 1540
  0.6 0.7 %copy-start.5 = (f32[1024]{0:T(1024)S(1)}, f32[1024]{0:T(1024)}, u32[]{:S(2)}) copy-start(f32[1024]{0:T(1024)} %param.10) | copy-start | bytes 12292
  0.7 0.7 %copy-start.7 = (f32[64]{0:T(128)S(1)}, f32[64]{0:T(128)}, u32[]{:S(2)}) copy-start(f32[64]{0:T(128)} %param.14) | copy-start | bytes 772
  0.7 0.7 %copy-start.8 = (f32[64]{0:T(128)S(1)}, f32[64]{0:T(128)}, u32[]{:S(2)}) copy-start(f32[64]{0:T(128)} %param.15) | copy-start | bytes 772
  1.3 1.2 %copy-start = (bf16[1024,512]{1,0:T(8,128)(2,1)S(1)}, bf16[1024,512]{1,0:T(8,128)(2,1)}, u32[]{:S(2)}) copy-start(bf16[1024,512]{1,0:T(8,128)(2,1)} %wq.1) | copy-start | bytes 3145732
  2.6 1.2 %copy-start.1 = (bf16[512,1024]{1,0:T(8,128)(2,1)S(1)}, bf16[512,1024]{1,0:T(8,128)(2,1)}, u32[]{:S(2)}) copy-start(bf16[512,1024]{1,0:T(8,128)(2,1)} %wo.1) | copy-start | bytes 3145732
  3.8 0.9 %copy-start.2 = (bf16[1,256,512]{2,1,0:T(8,128)(2,1)S(1)}, bf16[1,256,512]{2,1,0:T(8,128)(2,1)}, u32[]{:S(2)}) copy-start(bf16[1,256,512]{2,1,0:T(8,128)(2,1)} %param.9) | copy-start | bytes 786436
  4.7 0.9 %copy-start.3 = (bf16[1024,128]{1,0:T(8,128)(2,1)S(1)}, bf16[1024,128]{1,0:T(8,128)(2,1)}, u32[]{:S(2)}) copy-start(bf16[1024,128]{1,0:T(8,128)(2,1)} %wk.1) | copy-start | bytes 786436
  5.7 0.9 %copy-start.4 = (bf16[1024,128]{1,0:T(8,128)(2,1)S(1)}, bf16[1024,128]{1,0:T(8,128)(2,1)}, u32[]{:S(2)}) copy-start(bf16[1024,128]{1,0:T(8,128)(2,1)} %wv.1) | copy-start | bytes 786436

commit v2 on v1

--- a/solution.py
+++ b/solution.py
@@ -311,6 +311,17 @@
     out_ref[...] = (own + part_recv[...].astype(F32)).astype(BF16)
 
 
+def write_out(mixed, log_total, mixed_out, log_out, sems):
+    copies = [
+        pltpu.make_async_copy(mixed, mixed_out, sems.at[0]),
+        pltpu.make_async_copy(log_total, log_out, sems.at[1]),
+    ]
+    for copy in copies:
+        copy.start()
+    for copy in copies:
+        copy.wait()
+
+
 def shards(n_kv, tokens, norm_gain, w_query, w_key, w_value, q_gain, k_gain, w_out, chosen):
     seqs, rows, half = tokens.shape
     nb, entries = chosen.shape[1:]
@@ -324,7 +335,7 @@
             jax.ShapeDtypeStruct((rows, half), BF16),
             jax.ShapeDtypeStruct((heads, rows), F32),
         ),
-        in_specs=[pl.BlockSpec(memory_space=pl.ANY)] * 9,
+        in_specs=[pl.BlockSpec(memory_space=pltpu.HBM)] * 9,
         out_specs=(pl.BlockSpec(memory_space=vmem), pl.BlockSpec(memory_space=vmem)),
         scratch_shapes=[
             vmem((2, rows, half), BF16),
@@ -348,12 +359,22 @@
             dma((2,)),
         ],
         compiler_params=pltpu.CompilerParams(
-            collective_id=0, has_side_effects=True, vmem_limit_bytes=48 * 1024 * 1024
+            collective_id=0, has_side_effects=True, vmem_limit_bytes=66_000_000
         ),
     )(
         tokens.reshape(rows, half), norm_gain.reshape(1, -1), w_query, w_key, w_value,
         q_gain.reshape(1, -1), k_gain.reshape(1, -1), w_out, chosen.reshape(nb, entries),
     )
+    mixed, log_total = pl.pallas_call(
+        write_out,
+        out_shape=(
+            jax.ShapeDtypeStruct((rows, half), BF16),
+            jax.ShapeDtypeStruct((heads, rows), F32),
+        ),
+        in_specs=[pl.BlockSpec(memory_space=vmem)] * 2,
+        out_specs=(pl.BlockSpec(memory_space=pltpu.HBM),) * 2,
+        scratch_shapes=[dma((2,))],
+    )(mixed, log_total)
     return mixed.reshape(seqs, rows, half), log_total.reshape(seqs, heads, rows)
 
 

time: 25.3 us -> 20 us (0.79)
  local copies, waits for them, and re-layouts: 7.28 us -> 0 us
  Pallas kernels: 17.1 us -> 19.2 us
    unnamed x20 -> x0, local copies, waits for them, and re-layouts: 7.28 us -> none
    pallas_call x0 -> x1, Pallas kernels: none -> 1.67 us  [shards(): pl.pallas_call(write_out, out_shape=(jax.ShapeDtypeStruct((rows, half), B...]
    pallas_call x1, Pallas kernels: 17.1 us -> 17.6 us  [shards(): pl.pallas_call(functools.partial(kernel, n_kv), out_shape=(jax.ShapeDtype...]
where the time goes in v2:
time: 20 us; the launch traced here: 19.9 us
  Pallas kernels  19.2 us (96%)
  between operations  0.64 us (3%)
    pallas_call x1, Pallas kernels, shards(): pl.pallas_call(functools.partial(kernel, n_kv), out_shape=(jax.ShapeDtype...  17.6 us
    pallas_call x1, Pallas kernels, shards(): pl.pallas_call(write_out, out_shape=(jax.ShapeDtypeStruct((rows, half), B...  1.67 us

profile of v2, /device:TPU:19, one launch (start us, length us, event | category | flops | bytes accessed | tf_op | source)
XLA Modules:
  0.0 19.9 jit_solution(12038244751881227120)
XLA Ops:
  0.6 17.6 %shard_map.104 = (bf16[256,512]{1,0:T(8,128)(2,1)}, f32[8,256]{1,0:T(8,128)}) custom-call(bf16[256,512]{1,0:T(8,128)(2,1)} %bitcast.7, f32[1,1024]{1,0:T(1,128)} %bitcast.8, bf16[1024,512]{1,0:T(8,128)(2,1)} %wq.1, bf16[1024,128]{1,0:T(8,128)(2,1)} %wk.1, bf16[1024,128]{1,0:T(8,128)(2,1)} %wv.1, f32[1,64]{1,0:T(1,128)} %bitcast.10, f32[1,64]{1,0:T(1,128)} %bitcast.11, ...), custom_call_target="tpu_custom_call" | custom-call | tf_op jit(solution)/shard_map/pallas_call | solution.py:332
  18.2 1.7 %shard_map.105 = (bf16[256,512]{1,0:T(8,128)(2,1)}, f32[8,256]{1,0:T(8,128)}) custom-call(bf16[256,512]{1,0:T(8,128)(2,1)} %get-tuple-element.6.mixed, f32[8,256]{1,0:T(8,128)} %get-tuple-element.7.log_total), custom_call_target="tpu_custom_call" | custom-call | tf_op jit(solution)/shard_map/pallas_call | solution.py:368

commit v3 on v2

v3 whole, which is shorter than its diff:
```python
import functools
import math

import jax
import jax.numpy as jnp
from jax import lax
from jax.experimental import pallas as pl
from jax.experimental.pallas import tpu as pltpu
from jax.sharding import PartitionSpec as P

HD = 64
BLK = 32
MOST = 4
LANES = 128
PIECES = 3
PARTS = 2

epsilon = 1e-06
alibi_reach = 4.0
masked = -1e30
LOG2E = math.log2(math.e)
F32 = jnp.float32
BF16 = jnp.bfloat16
NT = (((1,), (1,)), ((), ()))


def iota(shape, dim):
    return lax.broadcasted_iota(jnp.int32, shape, dim)


def dot(a, b):
    return jnp.dot(a, b, preferred_element_type=F32)


def dot_nt(a, b):
    return lax.dot_general(a, b, NT, preferred_element_type=F32)


def kernel(
    n_kv,
    tok, gain, wq, wk, wv, qg, kg, wo, ch,
    out_ref, lt_ref,
    x_buf, ch_buf, code_send, code_recv, raw_s, w_buf, wo_buf, g_buf, qg_buf, kg_buf,
    q_s, kv_s, send_s, recv_s, acc, part_send, part_recv,
    load_sem, x_sem, ch_sem, kv_sem, part_sem,
):
    me = lax.axis_index("kv")
    tp = lax.axis_index("tp")
    partner = 1 - tp
    rows, half = tok.shape
    q_cols = wq.shape[1]
    k_cols = wk.shape[1]
    heads = q_cols // HD
    kv_heads = k_cols // HD
    group = heads // kv_heads
    n_heads = heads * lax.axis_size("tp")
    nb = ch.shape[0]
    entries = ch.shape[1]
    nbp = -(-n_kv * nb // LANES) * LANES
    picked = MOST * BLK
    width = half * 2
    seq_len = rows * n_kv
    alibi = alibi_reach / seq_len

    def span(start):
        return pl.ds(pl.multiple_of(start * half, LANES), half)

    loads = {}

    def load(name, src, dst):
        copy = pltpu.make_async_copy(src, dst, load_sem.at[len(loads)])
        copy.start()
        loads[name] = copy

    sides = ((0, tp), (1, partner))
    load("ch", ch, ch_buf)
    load("tok", tok, x_buf.at[0])
    load("g0", gain.at[:, span(tp)], g_buf.at[0])
    for side, which in sides:
        load(f"wk{side}", wk.at[span(which), :], w_buf.at[side, :, q_cols:q_cols + k_cols])
        load(f"wv{side}", wv.at[span(which), :], w_buf.at[side, :, q_cols + k_cols:q_cols + 2 * k_cols])
        load(f"wq{side}", wq.at[span(which), :], w_buf.at[side, :, 0:q_cols])
    load("g1", gain.at[:, span(partner)], g_buf.at[1])
    load("qg", qg, qg_buf)
    load("kg", kg, kg_buf)
    for side, which in sides:
        load(f"wo{side}", wo.at[:, span(which)], wo_buf.at[side])

    def peers(step):
        if n_kv <= 8:
            for d in range(1, n_kv):
                step(d)
        else:
            lax.fori_loop(1, n_kv, lambda d, c: (step(d), c)[1], 0)

    barrier = pltpu.get_barrier_semaphore()
    pl.semaphore_signal(barrier, inc=1, device_id={"tp": partner}, device_id_type=pl.DeviceIdType.MESH)
    peers(lambda d: pl.semaphore_signal(
        barrier, inc=1, device_id={"kv": lax.rem(me + d, n_kv)}, device_id_type=pl.DeviceIdType.MESH))

    loads["ch"].wait()
    lane_block = iota((nb, nbp), 1)
    lists = ch_buf[...]
    hit = lists[:, 0:1] == lane_block
    for e in range(1, entries):
        hit = hit | (lists[:, e:e + 1] == lane_block)
    member = jnp.where(hit, 1.0, 0.0)
    before = jnp.where(
        (iota((nbp, nbp), 0) < iota((nbp, nbp), 1))
        & (iota((nbp, nbp), 0) // nb == iota((nbp, nbp), 1) // nb), 1.0, 0.0).astype(BF16)
    need = jnp.broadcast_to(jnp.max(member, axis=0, keepdims=True), (8, nbp))
    place = jnp.where(need > 0.5, dot(need.astype(BF16), before), -1.0)

    def place_rows(owner):
        spread = jnp.where(
            iota((nbp, rows), 0) == owner * nb + iota((nbp, rows), 1) // BLK, 1.0, 0.0)
        return dot(place.astype(BF16), spread.astype(BF16))

    code_recv[me] = place_rows(me)

    def prepare_code(d):
        code_send[d] = place_rows(me - d)

    peers(prepare_code)

    def scaled(side):
        x = x_buf[side].astype(F32)
        return (x * g_buf[side]).astype(BF16), jnp.sum(x * x, axis=1, keepdims=True)

    for name in ("tok", "g0", "wk0", "wv0", "wq0"):
        loads[name].wait()
    y0, sq0 = scaled(0)
    raw_s[...] = dot(y0, w_buf[0])
    pl.semaphore_wait(barrier, n_kv)

    x_copy = pltpu.make_async_remote_copy(
        x_buf.at[0], x_buf.at[1], x_sem.at[0], x_sem.at[1],
        device_id={"tp": partner}, device_id_type=pl.DeviceIdType.MESH)
    x_copy.start()

    def code_copy(owner, target, d):
        return pltpu.make_async_remote_copy(
            code_send.at[d], code_recv.at[owner], ch_sem.at[0, target], ch_sem.at[1, owner],
            device_id={"kv": target}, device_id_type=pl.DeviceIdType.MESH)

    def send_code(d):
        @pl.when(me - d >= 0)
        def _():
            code_copy(me, lax.max(me - d, 0), d).start()

    peers(send_code)

    same_head = jnp.where(
        iota((LANES, LANES), 0) // HD == iota((LANES, LANES), 1) // HD, 1.0, 0.0).astype(BF16)

    def head_norm(v, gain_row):
        sq = v * v
        hi = sq.astype(BF16)
        lo = (sq - hi.astype(F32)).astype(BF16)
        total = dot(hi, same_head) + dot(lo, same_head)
        return v * lax.rsqrt(total / HD + epsilon) * gain_row

    for name in ("g1", "qg", "kg", "wk1", "wv1", "wq1"):
        loads[name].wait()
    qg_row = jnp.concatenate([qg_buf[...], qg_buf[...]], axis=1) * (HD ** -0.5 * LOG2E)
    kg_row = jnp.concatenate([kg_buf[...], kg_buf[...]], axis=1)
    x_copy.wait()
    y1, sq1 = scaled(1)
    row_scale = lax.rsqrt((sq0 + sq1) / width + epsilon)
    raw_kv = (raw_s[:, q_cols:] + dot(y1, w_buf[1, :, q_cols:])) * row_scale
    for tile in range(k_cols // LANES):
        at = tile * LANES
        kv_s[:, at:at + LANES] = head_norm(raw_kv[:, at:at + LANES], kg_row).astype(BF16)
    kv_s[:, k_cols:] = raw_kv[:, k_cols:].astype(BF16)

    same_row = iota((picked, rows), 0) % BLK == iota((picked, rows), 1) % BLK
    row_slot = (iota((picked, rows), 0) // BLK).astype(F32)

    def kv_copy(owner, target, d):
        return pltpu.make_async_remote_copy(
            send_s.at[d], recv_s.at[owner], kv_sem.at[0, target], kv_sem.at[1, owner],
            device_id={"kv": target}, device_id_type=pl.DeviceIdType.MESH)

    def await_code(d):
        @pl.when(me + d < n_kv)
        def _():
            code_copy(lax.min(me + d, n_kv - 1), me, d).wait_recv()

    def pack(d):
        code = code_recv[lax.min(me + d, n_kv - 1)][0:1]
        chosen_rows = jnp.where(same_row & (code == row_slot), 1.0, 0.0).astype(BF16)
        send_s[d] = dot(chosen_rows, kv_s[...]).astype(BF16)

    def send_rows(step):
        d = n_kv - step

        @pl.when(me + d < n_kv)
        def _():
            kv_copy(me, lax.min(me + d, n_kv - 1), d).start()

    peers(await_code)
    peers(pack)
    peers(send_rows)
    raw = (raw_s[:, 0:q_cols] + dot(y1, w_buf[1, :, 0:q_cols])) * row_scale

    lane_q = iota((rows, LANES), 1)
    row_q = iota((rows, LANES), 0)
    own_block = jnp.where(lane_q - HD == row_q // BLK, 1.0, 0.0)

    def slope_of(head):
        return jnp.exp2(-8.0 / n_heads * (tp * heads + head + 1).astype(F32))

    def lane_fill(base, first, value):
        return jnp.where(lane_q == first, value, base)

    for tile in range(q_cols // LANES):
        at = tile * LANES
        q = head_norm(raw[:, at:at + LANES], qg_row)
        for odd in range(2):
            head = 2 * tile + odd
            value = slope_of(jnp.full((rows, LANES), head, jnp.int32)) * (alibi * LOG2E)
            extra = own_block
            for piece in range(PIECES):
                part = value.astype(BF16).astype(F32)
                value = value - part
                extra = lane_fill(extra, HD + nb + piece, part * BLK)
                extra = lane_fill(extra, HD + nb + PIECES + piece, part)
            here = q if odd == 0 else pltpu.roll(q, HD, 1)
            q_s[head] = jnp.where(lane_q < HD, here, extra).astype(BF16)

    relative = (lane_block - me * nb).astype(F32)
    pieces_rows = jnp.where(
        iota((8, nbp), 0) < PIECES,
        jnp.broadcast_to(relative[0:1], (8, nbp)), 0.0)
    table = jnp.concatenate(
        [jnp.zeros((HD, nbp), F32), member, pieces_rows,
         jnp.zeros((LANES - HD - nb - 8, nbp), F32)], axis=0).astype(BF16)

    def key_extra(hot):
        count = hot.shape[0]
        lane = iota((count, LANES), 1)
        found = dot_nt(hot, table)
        inside = (iota((count, LANES), 0) % BLK).astype(F32)
        tail = jnp.where(lane < HD + nb + 2 * PIECES, inside, 0.0)
        tail = jnp.where(lane < HD + nb + PIECES, found, tail)
        return jnp.where(lane < HD + nb, (found - 1.0) * -masked, tail)

    def attend(load_tile, extra, causal, first):
        count = extra.shape[0]
        low = iota((count, LANES), 1) < HD
        for g in range(kv_heads):
            at = g * HD // LANES * LANES
            k = load_tile(at).astype(F32)
            v = load_tile(k_cols + at).astype(F32)
            if g % 2:
                k = pltpu.roll(k, HD, 1)
                v = pltpu.roll(v, HD, 1)
            k = jnp.where(low, k, extra).astype(BF16)
            v = jnp.where(low, v, 1.0).astype(BF16)
            for h in range(g * group, (g + 1) * group):
                weights = jnp.exp2(dot_nt(q_s[h], k))
                if causal is not None:
                    weights = jnp.where(causal, weights, 0.0)
                add = dot(weights.astype(BF16), v)
                if first:
                    acc[h] = add
                else:
                    acc[h] += add

    hot_own = jnp.where(
        iota((rows, nbp), 1) == me * nb + iota((rows, nbp), 0) // BLK, 1.0, 0.0).astype(BF16)
    causal = iota((rows, rows), 1) <= iota((rows, rows), 0)
    attend(lambda at: kv_s[:, at:at + LANES], key_extra(hot_own), causal, True)

    slot = (iota((picked, nbp), 0) // BLK).astype(F32)
    lane_owner = iota((picked, nbp), 1) // nb

    def absorb(d):
        @pl.when(me - d >= 0)
        def _():
            owner = lax.max(me - d, 0)
            hot = jnp.where((place[0:1] == slot) & (lane_owner == owner), 1.0, 0.0)
            extra = key_extra(hot.astype(BF16))
            kv_copy(owner, me, d).wait_recv()
            attend(lambda at: recv_s[owner, :, at:at + LANES], extra, None, False)

    peers(absorb)

    loads["wo0"].wait()
    loads["wo1"].wait()
    part_rows = rows // PARTS
    low = iota((part_rows, LANES), 1) < HD
    lane = iota((part_rows, LANES), 1)

    def part_copy(part):
        at = pl.ds(part * part_rows, part_rows)
        return pltpu.make_async_remote_copy(
            part_send.at[at], part_recv.at[at], part_sem.at[0, part], part_sem.at[1, part],
            device_id={"tp": partner}, device_id_type=pl.DeviceIdType.MESH)

    attended, all_sums = [], []
    for part in range(PARTS):
        at = slice(part * part_rows, (part + 1) * part_rows)
        sums = jnp.ones((part_rows, LANES), F32)
        tiles = []
        for tile in range(q_cols // LANES):
            pair = []
            for odd in range(2):
                head = 2 * tile + odd
                o = acc[head, at]
                total = pltpu.roll(o, HD, 1)
                sums = jnp.where(lane == head, total, sums)
                pair.append(o / total)
            tiles.append(jnp.where(low, pair[0], pltpu.roll(pair[1], HD, 1)))
        attended.append(jnp.concatenate(tiles, axis=1).astype(BF16))
        all_sums.append(sums)
        part_send[at] = dot(attended[part], wo_buf[1]).astype(BF16)
        part_copy(part).start()

    own = [dot(a, wo_buf[0]) for a in attended]
    logs = jnp.log(jnp.concatenate(all_sums, axis=0))
    logs = logs - slope_of(lane_q) * alibi * row_q.astype(F32)
    lt_ref[...] = logs.T[0:heads]

    def finish(d):
        @pl.when(me + d < n_kv)
        def _():
            kv_copy(me, lax.min(me + d, n_kv - 1), d).wait_send()

        @pl.when(me - d >= 0)
        def _():
            code_copy(me, lax.max(me - d, 0), d).wait_send()

    peers(finish)
    for part in range(PARTS):
        at = slice(part * part_rows, (part + 1) * part_rows)
        part_copy(part).wait()
        out_ref[at] = (own[part] + part_recv[at].astype(F32)).astype(BF16)


def write_out(mixed, log_total, mixed_out, log_out, sems):
    copies = [
        pltpu.make_async_copy(mixed, mixed_out, sems.at[0]),
        pltpu.make_async_copy(log_total, log_out, sems.at[1]),
    ]
    for copy in copies:
        copy.start()
    for copy in copies:
        copy.wait()


def shards(n_kv, tokens, norm_gain, w_query, w_key, w_value, q_gain, k_gain, w_out, chosen):
    seqs, rows, half = tokens.shape
    nb, entries = chosen.shape[1:]
    q_cols, k_cols = w_query.shape[1], w_key.shape[1]
    heads = q_cols // HD
    vmem = pltpu.VMEM
    dma = pltpu.SemaphoreType.DMA
    mixed, log_total = pl.pallas_call(
        functools.partial(kernel, n_kv),
        out_shape=(vmem((rows, half), BF16), vmem((heads, rows), F32)),
        in_specs=[pl.BlockSpec(memory_space=pltpu.HBM)] * 9,
        out_specs=(pl.BlockSpec(memory_space=vmem), pl.BlockSpec(memory_space=vmem)),
        scratch_shapes=[
            vmem((2, rows, half), BF16),
            vmem((nb, entries), jnp.int32),
            vmem((n_kv, 8, rows), F32),
            vmem((n_kv, 8, rows), F32),
            vmem((rows, q_cols + 2 * k_cols), F32),
            vmem((2, half, q_cols + 2 * k_cols), BF16),
            vmem((2, q_cols, half), BF16),
            vmem((2, 1, half), F32),
            vmem((1, HD), F32),
            vmem((1, HD), F32),
            vmem((heads, rows, LANES), BF16),
            vmem((rows, 2 * k_cols), BF16),
            vmem((n_kv, MOST * BLK, 2 * k_cols), BF16),
            vmem((n_kv, MOST * BLK, 2 * k_cols), BF16),
            vmem((heads, rows, LANES), F32),
            vmem((rows, half), BF16),
            vmem((rows, half), BF16),
            dma((14,)),
            dma((2,)),
            dma((2, n_kv)),
            dma((2, n_kv)),
            dma((2, PARTS)),
        ],
        compiler_params=pltpu.CompilerParams(
            collective_id=0, has_side_effects=True, vmem_limit_bytes=66_700_000
        ),
    )(
        tokens.reshape(rows, half), norm_gain.reshape(1, -1), w_query, w_key, w_value,
        q_gain.reshape(1, -1), k_gain.reshape(1, -1), w_out, chosen.reshape(nb, entries),
    )
    mixed, log_total = pl.pallas_call(
        write_out,
        out_shape=(
            jax.ShapeDtypeStruct((rows, half), BF16),
            jax.ShapeDtypeStruct((heads, rows), F32),
        ),
        in_specs=[pl.BlockSpec(memory_space=pl.ANY)] * 2,
        out_specs=(pl.BlockSpec(memory_space=pltpu.HBM),) * 2,
        scratch_shapes=[dma((2,))],
        compiler_params=pltpu.CompilerParams(vmem_limit_bytes=1_000_000),
    )(mixed, log_total)
    return mixed.reshape(seqs, rows, half), log_total.reshape(seqs, heads, rows)


def solution(mesh):
    in_specs = (
        P("dp", "kv", "tp"),
        P(),
        P(None, "tp"),
        P(None, "tp"),
        P(None, "tp"),
        P(),
        P(),
        P("tp", None),
        P("dp", "kv", None),
    )
    out_specs = (P("dp", "kv", "tp"), P("dp", "tp", "kv"))
    return jax.shard_map(
        functools.partial(shards, mesh.shape["kv"]),
        mesh=mesh, in_specs=in_specs, out_specs=out_specs, check_vma=False)
```

time: 20 us -> 17.9 us (0.89)
  Pallas kernels: 19.2 us -> 17 us
    pallas_call x1, Pallas kernels: 17.6 us -> 16.3 us  [shards(): pl.pallas_call(functools.partial(kernel, n_kv), out_shape=(vmem((rows, ha...]
    pallas_call x1, Pallas kernels: 1.67 us -> 0.72 us  [shards(): pl.pallas_call(write_out, out_shape=(jax.ShapeDtypeStruct((rows, half), B...]
where the time goes in v3:
time: 17.9 us; the launch traced here: 17.7 us
  Pallas kernels  17 us (95%)
  between operations  0.64 us (4%)
    pallas_call x1, Pallas kernels, shards(): pl.pallas_call(functools.partial(kernel, n_kv), out_shape=(vmem((rows, ha...  16.3 us
    pallas_call x1, Pallas kernels, shards(): pl.pallas_call(write_out, out_shape=(jax.ShapeDtypeStruct((rows, half), B...  0.72 us

profile of v3, /device:TPU:19, one launch (start us, length us, event | category | flops | bytes accessed | tf_op | source)
XLA Modules:
  0.0 17.7 jit_solution(4366174070241617229)
XLA Ops:
  0.6 16.3 %shard_map.104 = (bf16[256,512]{1,0:T(8,128)(2,1)S(1)}, f32[8,256]{1,0:T(8,128)S(1)}) custom-call(bf16[256,512]{1,0:T(8,128)(2,1)} %bitcast.7, f32[1,1024]{1,0:T(1,128)} %bitcast.8, bf16[1024,512]{1,0:T(8,128)(2,1)} %wq.1, bf16[1024,128]{1,0:T(8,128)(2,1)} %wk.1, bf16[1024,128]{1,0:T(8,128)(2,1)} %wv.1, f32[1,64]{1,0:T(1,128)} %bitcast.10, ...), custom_call_target="tpu_custom_call" | custom-call | tf_op jit(solution)/shard_map/pallas_call | solution.py:359
  17.0 0.7 %shard_map.105 = (bf16[256,512]{1,0:T(8,128)(2,1)}, f32[8,256]{1,0:T(8,128)}) custom-call(bf16[256,512]{1,0:T(8,128)(2,1)S(1)} %get-tuple-element.6.mixed, f32[8,256]{1,0:T(8,128)S(1)} %get-tuple-element.7.log_total), custom_call_target="tpu_custom_call" | custom-call | tf_op jit(solution)/shard_map/pallas_call | solution.py:395

commit v4 on v3

--- a/solution.py
+++ b/solution.py
@@ -93,6 +93,9 @@
         else:
             lax.fori_loop(1, n_kv, lambda d, c: (step(d), c)[1], 0)
 
+    def far_first(step):
+        peers(lambda d: step(n_kv - d))
+
     barrier = pltpu.get_barrier_semaphore()
     pl.semaphore_signal(barrier, inc=1, device_id={"tp": partner}, device_id_type=pl.DeviceIdType.MESH)
     peers(lambda d: pl.semaphore_signal(
@@ -116,8 +119,6 @@
             iota((nbp, rows), 0) == owner * nb + iota((nbp, rows), 1) // BLK, 1.0, 0.0)
         return dot(place.astype(BF16), spread.astype(BF16))
 
-    code_recv[me] = place_rows(me)
-
     def prepare_code(d):
         code_send[d] = place_rows(me - d)
 
@@ -133,22 +134,22 @@
     raw_s[...] = dot(y0, w_buf[0])
     pl.semaphore_wait(barrier, n_kv)
 
+    def code_copy(owner, target, d):
+        return pltpu.make_async_remote_copy(
+            code_send.at[d], code_recv.at[owner], ch_sem.at[0, target], ch_sem.at[1, owner],
+            device_id={"kv": target}, device_id_type=pl.DeviceIdType.MESH)
+
+    def send_code(d):
+        @pl.when(me - d >= 0)
+        def _():
+            code_copy(me, lax.max(me - d, 0), d).start()
+
+    peers(send_code)
+
     x_copy = pltpu.make_async_remote_copy(
         x_buf.at[0], x_buf.at[1], x_sem.at[0], x_sem.at[1],
         device_id={"tp": partner}, device_id_type=pl.DeviceIdType.MESH)
     x_copy.start()
-
-    def code_copy(owner, target, d):
-        return pltpu.make_async_remote_copy(
-            code_send.at[d], code_recv.at[owner], ch_sem.at[0, target], ch_sem.at[1, owner],
-            device_id={"kv": target}, device_id_type=pl.DeviceIdType.MESH)
-
-    def send_code(d):
-        @pl.when(me - d >= 0)
-        def _():
-            code_copy(me, lax.max(me - d, 0), d).start()
-
-    peers(send_code)
 
     same_head = jnp.where(
         iota((LANES, LANES), 0) // HD == iota((LANES, LANES), 1) // HD, 1.0, 0.0).astype(BF16)
@@ -181,26 +182,17 @@
             send_s.at[d], recv_s.at[owner], kv_sem.at[0, target], kv_sem.at[1, owner],
             device_id={"kv": target}, device_id_type=pl.DeviceIdType.MESH)
 
-    def await_code(d):
+    def send_rows(d):
         @pl.when(me + d < n_kv)
         def _():
-            code_copy(lax.min(me + d, n_kv - 1), me, d).wait_recv()
-
-    def pack(d):
-        code = code_recv[lax.min(me + d, n_kv - 1)][0:1]
-        chosen_rows = jnp.where(same_row & (code == row_slot), 1.0, 0.0).astype(BF16)
-        send_s[d] = dot(chosen_rows, kv_s[...]).astype(BF16)
-
-    def send_rows(step):
-        d = n_kv - step
-
-        @pl.when(me + d < n_kv)
-        def _():
-            kv_copy(me, lax.min(me + d, n_kv - 1), d).start()
-
-    peers(await_code)
-    peers(pack)
-    peers(send_rows)
+            target = lax.min(me + d, n_kv - 1)
+            code_copy(target, me, d).wait_recv()
+            code = code_recv[target][0:1]
+            chosen_rows = jnp.where(same_row & (code == row_slot), 1.0, 0.0).astype(BF16)
+            send_s[d] = dot(chosen_rows, kv_s[...]).astype(BF16)
+            kv_copy(me, target, d).start()
+
+    far_first(send_rows)
     raw = (raw_s[:, 0:q_cols] + dot(y1, w_buf[1, :, 0:q_cols])) * row_scale
 
     lane_q = iota((rows, LANES), 1)
@@ -284,7 +276,7 @@
             kv_copy(owner, me, d).wait_recv()
             attend(lambda at: recv_s[owner, :, at:at + LANES], extra, None, False)
 
-    peers(absorb)
+    far_first(absorb)
 
     loads["wo0"].wait()
     loads["wo1"].wait()
@@ -306,12 +298,12 @@
         for tile in range(q_cols // LANES):
             pair = []
             for odd in range(2):
-                head = 2 * tile + odd
-                o = acc[head, at]
-                total = pltpu.roll(o, HD, 1)
-                sums = jnp.where(lane == head, total, sums)
-                pair.append(o / total)
-            tiles.append(jnp.where(low, pair[0], pltpu.roll(pair[1], HD, 1)))
+                pair.append(acc[2 * tile + odd, at])
+            turned = [pltpu.roll(o, HD, 1) for o in pair]
+            total = jnp.where(low, turned[0], pair[1])
+            tiles.append(jnp.where(low, pair[0], turned[1]) / total)
+            for odd in range(2):
+                sums = jnp.where(lane == 2 * tile + odd, turned[odd], sums)
         attended.append(jnp.concatenate(tiles, axis=1).astype(BF16))
         all_sums.append(sums)
         part_send[at] = dot(attended[part], wo_buf[1]).astype(BF16)

time: 17.9 us -> 16.9 us (0.944)
  Pallas kernels: 17 us -> 16.1 us
    pallas_call x1, Pallas kernels: 16.3 us -> 15.4 us  [shards(): pl.pallas_call(functools.partial(kernel, n_kv), out_shape=(vmem((rows, ha...]
where the time goes in v4:
time: 16.9 us; the launch traced here: 16.8 us
  Pallas kernels  16.1 us (95%)
  between operations  0.64 us (4%)
    pallas_call x1, Pallas kernels, shards(): pl.pallas_call(functools.partial(kernel, n_kv), out_shape=(vmem((rows, ha...  15.4 us
    pallas_call x1, Pallas kernels, shards(): pl.pallas_call(write_out, out_shape=(jax.ShapeDtypeStruct((rows, half), B...  0.72 us

profile of v4, /device:TPU:19, one launch (start us, length us, event | category | flops | bytes accessed | tf_op | source)
XLA Modules:
  0.0 16.8 jit_solution(5957068276404268630)
XLA Ops:
  0.6 15.4 %shard_map.104 = (bf16[256,512]{1,0:T(8,128)(2,1)S(1)}, f32[8,256]{1,0:T(8,128)S(1)}) custom-call(bf16[256,512]{1,0:T(8,128)(2,1)} %bitcast.7, f32[1,1024]{1,0:T(1,128)} %bitcast.8, bf16[1024,512]{1,0:T(8,128)(2,1)} %wq.1, bf16[1024,128]{1,0:T(8,128)(2,1)} %wk.1, bf16[1024,128]{1,0:T(8,128)(2,1)} %wv.1, f32[1,64]{1,0:T(1,128)} %bitcast.10, ...), custom_call_target="tpu_custom_call" | custom-call | tf_op jit(solution)/shard_map/pallas_call | solution.py:351
  16.0 0.7 %shard_map.105 = (bf16[256,512]{1,0:T(8,128)(2,1)}, f32[8,256]{1,0:T(8,128)}) custom-call(bf16[256,512]{1,0:T(8,128)(2,1)S(1)} %get-tuple-element.6.mixed, f32[8,256]{1,0:T(8,128)S(1)} %get-tuple-element.7.log_total), custom_call_target="tpu_custom_call" | custom-call | tf_op jit(solution)/shard_map/pallas_call | solution.py:387

commit v5 on v4

--- a/solution.py
+++ b/solution.py
@@ -131,7 +131,7 @@
     for name in ("tok", "g0", "wk0", "wv0", "wq0"):
         loads[name].wait()
     y0, sq0 = scaled(0)
-    raw_s[...] = dot(y0, w_buf[0])
+    raw_s[:, q_cols:] = dot(y0, w_buf[0, :, q_cols:])
     pl.semaphore_wait(barrier, n_kv)
 
     def code_copy(owner, target, d):
@@ -193,7 +193,7 @@
             kv_copy(me, target, d).start()
 
     far_first(send_rows)
-    raw = (raw_s[:, 0:q_cols] + dot(y1, w_buf[1, :, 0:q_cols])) * row_scale
+    raw = (dot(y0, w_buf[0, :, 0:q_cols]) + dot(y1, w_buf[1, :, 0:q_cols])) * row_scale
 
     lane_q = iota((rows, LANES), 1)
     row_q = iota((rows, LANES), 0)
@@ -323,11 +323,11 @@
         def _():
             code_copy(me, lax.max(me - d, 0), d).wait_send()
 
-    peers(finish)
     for part in range(PARTS):
         at = slice(part * part_rows, (part + 1) * part_rows)
         part_copy(part).wait()
         out_ref[at] = (own[part] + part_recv[at].astype(F32)).astype(BF16)
+    peers(finish)
 
 
 def write_out(mixed, log_total, mixed_out, log_out, sems):

time: 16.9 us -> 16.8 us (level)
  no operation moved by 1% of the time
where the time goes in v5:
time: 16.8 us; the launch traced here: 16.6 us
  Pallas kernels  16 us (95%)
  between operations  0.64 us (4%)
    pallas_call x1, Pallas kernels, shards(): pl.pallas_call(functools.partial(kernel, n_kv), out_shape=(vmem((rows, ha...  15.3 us
    pallas_call x1, Pallas kernels, shards(): pl.pallas_call(write_out, out_shape=(jax.ShapeDtypeStruct((rows, half), B...  0.72 us

profile of v5, /device:TPU:19, one launch (start us, length us, event | category | flops | bytes accessed | tf_op | source)
XLA Modules:
  0.0 16.6 jit_solution(11254685348209953147)
XLA Ops:
  0.6 15.3 %shard_map.104 = (bf16[256,512]{1,0:T(8,128)(2,1)S(1)}, f32[8,256]{1,0:T(8,128)S(1)}) custom-call(bf16[256,512]{1,0:T(8,128)(2,1)} %bitcast.7, f32[1,1024]{1,0:T(1,128)} %bitcast.8, bf16[1024,512]{1,0:T(8,128)(2,1)} %wq.1, bf16[1024,128]{1,0:T(8,128)(2,1)} %wk.1, bf16[1024,128]{1,0:T(8,128)(2,1)} %wv.1, f32[1,64]{1,0:T(1,128)} %bitcast.10, ...), custom_call_target="tpu_custom_call" | custom-call | tf_op jit(solution)/shard_map/pallas_call | solution.py:351
  15.9 0.7 %shard_map.105 = (bf16[256,512]{1,0:T(8,128)(2,1)}, f32[8,256]{1,0:T(8,128)}) custom-call(bf16[256,512]{1,0:T(8,128)(2,1)S(1)} %get-tuple-element.6.mixed, f32[8,256]{1,0:T(8,128)S(1)} %get-tuple-element.7.log_total), custom_call_target="tpu_custom_call" | custom-call | tf_op jit(solution)/shard_map/pallas_call | solution.py:387
